TPU v7x, 32 devices: a whole 2x2x4 slice. The times are simulated.
32 devices in a mesh: grp: 2 (over y), ep: 8 (over z, x), tp: 2 (over core).
Axes of the slice: x: 2, y: 2, z: 4, core: 2. Of those that a mesh axis runs over, the one named last changes fastest.
Arguments:
- tokens: bfloat16 [1024, 2048], P(('grp', 'ep')), parts along dimension 0, may hold values from -6 to 6
- chosen: int32 [1, 16, 9], P(None, ('grp', 'ep')), parts along dimension 1, may hold values from -1 to 63, as said below
- route_weight: float32 [1, 16, 9], P(None, ('grp', 'ep')), parts along dimension 1, may hold values from 0.1 to 1
- expert_gate: bfloat16 [2048, 4096], P(None, ('ep', 'tp')), may hold values from -0.125 to 0.125
- expert_up: bfloat16 [2048, 4096], P(None, ('ep', 'tp')), may hold values from -0.125 to 0.125
- expert_down: bfloat16 [4096, 2048], P(('ep', 'tp')), may hold values from -0.09375 to 0.09375
- dense_gate: bfloat16 [2048, 512], P('ep', 'tp'), may hold values from -0.125 to 0.125
- dense_up: bfloat16 [2048, 512], P('ep', 'tp'), may hold values from -0.125 to 0.125
- dense_down: bfloat16 [512, 2048], P('tp', 'ep'), may hold values from -0.25 to 0.25
- branch_gate: float32 [2048], P('tp'), may hold values from -6 to 6
Outputs:
- mixed: bfloat16 [1024, 2048], P(('grp', 'ep'), 'tp'), parts along dimension 0
There are 2 independent parts, one for each index of `grp`. A program takes and returns all parts, laid end to end along the dimension named above; an argument that names none is the same for every part. Nothing has to cross between parts.
Inputs may be any that keep to these rules, and one draw needn't show every extreme that they name: chosen[e, s, k] is -1 or an index local to device s (token s * 64 + chosen[e, s, k] of the whole). In each (e, s) row the live entries come first and are distinct, the -1 entries follow. Each expert takes exactly 64 tokens in all, at most 9 from one device, and for every expert some device gives it exactly 9.
All inputs are finite; a program needn't handle non-finite values.
Results may differ from a plain program's by a relative error of at most 0.0085.
Values may be sent and summed in bfloat16 or wider, within the bound.
A program may use at most 64 MiB of HBM per device.

v0:
```python
import jax
import jax.numpy as jnp
from jax import lax
from jax.sharding import PartitionSpec as P


def swapped(block, axis, apart):
    count = lax.axis_size(axis)
    route = []
    for low in range(count):
        high = low | 1 << apart
        if high != low and high < count:
            route += [(low, high), (high, low)]
    return lax.ppermute(block, axis, route)


def expert_hidden(received, gate_cols, up_cols):
    flat_rows = received.reshape(-1, received.shape[-1])
    gate_act = jnp.dot(flat_rows, gate_cols, preferred_element_type=jnp.float32)
    up_act = jnp.dot(flat_rows, up_cols, preferred_element_type=jnp.float32)
    hidden = (jax.nn.silu(gate_act) * up_act).astype(jnp.bfloat16)
    return hidden.reshape(received.shape[0], received.shape[1], gate_cols.shape[1])


def join_pieces(mine, theirs, upper):
    return jnp.where(upper, jnp.concatenate([theirs, mine], 2), jnp.concatenate([mine, theirs], 2))


def local(
    tokens,
    chosen,
    route_weight,
    expert_gate,
    expert_up,
    expert_down,
    dense_gate,
    dense_up,
    dense_down,
    branch_gate,
):
    ep_count = lax.axis_size("ep")
    experts = chosen.shape[0]
    slots = chosen.shape[2]
    tok_local = tokens.shape[0]
    width = tokens.shape[1]
    picked = chosen[:, 0, :]
    filled = picked >= 0
    token_rows = jnp.take(tokens, jnp.maximum(picked, 0).reshape(-1), axis=0).reshape(
        experts, slots, width
    )
    token_rows = jnp.where(filled[:, :, None], token_rows, jnp.zeros((), jnp.bfloat16))
    send_width = token_rows.shape[2]
    piece = send_width // 8
    split_rows = jnp.transpose(token_rows.reshape(experts, slots, 8, piece), (0, 2, 1, 3)).reshape(
        ep_count, slots, piece
    )
    own_piece = lax.all_to_all(split_rows, "ep", split_axis=0, concat_axis=0, tiled=True)
    member = lax.axis_index("ep") % 8
    current = own_piece[:, :, None, :]
    partner = swapped(current, "ep", 0)
    current = join_pieces(current, partner, member % 2 == 1)
    partner = swapped(current, "ep", 1)
    current = join_pieces(current, partner, member // 2 % 2 == 1)
    partner = swapped(current, "ep", 2)
    current = join_pieces(current, partner, member // 4 == 1)
    received = current.reshape(ep_count, slots, send_width)
    hidden = expert_hidden(received, gate_cols=expert_gate, up_cols=expert_up)
    flat_hidden = hidden.reshape(ep_count * slots, -1)
    shard_rows = expert_down
    member_sums = lax.psum_scatter(
        lax.dot_general(
            shard_rows, flat_hidden, (((0,), (1,)), ((), ())), preferred_element_type=jnp.float32
        ).astype(jnp.bfloat16),
        "tp",
        scatter_dimension=0,
        tiled=True,
    )
    returned = lax.all_to_all(member_sums, "ep", split_axis=1, concat_axis=1, tiled=True)
    summed = returned.astype(jnp.float32).reshape(width // 2, experts, 8, slots).sum(axis=2)
    positions = lax.broadcasted_iota(jnp.int32, (experts, slots, tok_local), 2)
    weights_table = jnp.where(picked[:, :, None] == positions, route_weight[:, 0, :, None], 0.0)
    combined = jnp.einsum("fek,ekt->tf", summed, weights_table, precision=lax.Precision.HIGHEST)
    shard_rows = (
        lax.all_gather(dense_gate, "ep", axis=0, tiled=True),
        lax.all_gather(dense_up, "ep", axis=0, tiled=True),
    )
    gate_dense = jnp.dot(tokens, shard_rows[0], preferred_element_type=jnp.float32)
    up_dense = jnp.dot(tokens, shard_rows[1], preferred_element_type=jnp.float32)
    dense_hidden = (jax.nn.silu(gate_dense) * up_dense).astype(jnp.bfloat16)
    dense_terms = jnp.dot(
        dense_hidden,
        lax.all_gather(dense_down, "ep", axis=1, tiled=True),
        preferred_element_type=jnp.float32,
    )
    dense_sum = lax.psum_scatter(
        dense_terms.astype(jnp.bfloat16), "tp", scatter_dimension=1, tiled=True
    ).astype(jnp.float32)
    return (combined + jax.nn.sigmoid(branch_gate)[None, :] * dense_sum).astype(jnp.bfloat16)


def solution(mesh):
    return jax.shard_map(
        local,
        mesh=mesh,
        in_specs=(
            P(("grp", "ep"), None),
            P(None, ("grp", "ep"), None),
            P(None, ("grp", "ep"), None),
            P(None, ("ep", "tp")),
            P(None, ("ep", "tp")),
            P(("ep", "tp"), None),
            P("ep", "tp"),
            P("ep", "tp"),
            P("tp", "ep"),
            P("tp"),
        ),
        out_specs=P(("grp", "ep"), "tp"),
        check_vma=False,
    )
```

profile of v0, /device:TPU:0, one launch (start us, length us, event | category | flops | bytes accessed | tf_op | source)
XLA Modules:
  0.0 162.1 jit_solution(17605187083843992932)
XLA Ops:
  7.4 0.7 all-gather.4.cloned.1.call-update
  8.1 0.7 all-gather.6.cloned.1.call-update
  8.9 0.7 all-gather.8.cloned.1.call-update
  9.7 0.6 gather_fusion
  10.3 0.1 fusion.10
  10.4 14.1 %all_to_all.14 = bf16[8,9,256]{2,1,0:T(8,128)(2,1)S(1)} all-to-all(bf16[8,9,256]{2,1,0:T(8,128)(2,1)S(1)} %fusion.10), channel_id=1, replica_groups=mesh['grp'=2,'ep'=8,'tp'=2] {'ep'}, dimensions={0} | all-to-all | bytes 73728 | tf_op jit(solution)/shard_map/all_to_all | solution.py:57
  24.5 0.4 collective-permute-start
  24.9 3.7 %collective-permute-done = bf16[8,9,1,256]{3,0,2,1:T(8,128)(2,1)S(1)} collective-permute-done((bf16[8,9,1,256]{3,0,2,1:T(8,128)(2,1)S(1)}, bf16[8,9,1,256]{3,0,2,1:T(8,128)(2,1)S(1)}, u32[]{:S(2)}, u32[]{:S(2)}) %collective-permute-start) | collective-permute-done | bytes 36896 | tf_op jit(solution)/shard_map/ppermute | solution.py:14
  28.5 0.2 collective-permute-start.1
  28.7 4.7 %collective-permute-done.1 = bf16[8,9,2,256]{3,0,2,1:T(8,128)(2,1)S(1)} collective-permute-done((bf16[8,9,2,256]{3,0,2,1:T(8,128)(2,1)S(1)}, bf16[8,9,2,256]{3,0,2,1:T(8,128)(2,1)S(1)}, u32[]{:S(2)}, u32[]{:S(2)}) %collective-permute-start.1) | collective-permute-done | bytes 73760 | tf_op jit(solution)/shard_map/ppermute | solution.py:14
  33.5 0.5 collective-permute-start.2
  34.0 6.7 %collective-permute-done.2 = bf16[8,9,4,256]{3,0,2,1:T(8,128)(2,1)S(1)} collective-permute-done((bf16[8,9,4,256]{3,0,2,1:T(8,128)(2,1)S(1)}, bf16[8,9,4,256]{3,0,2,1:T(8,128)(2,1)S(1)}, u32[]{:S(2)}, u32[]{:S(2)}) %collective-permute-start.2) | collective-permute-done | bytes 147488 | tf_op jit(solution)/shard_map/ppermute | solution.py:14
  40.9 0.3 fusion.25
  41.2 2.7 %fusion = bf16[2048,72]{0,1:T(8,128)(2,1)} fusion(bf16[256,2048]{1,0:T(8,128)(2,1)S(1)} %copy-done, bf16[72,2048]{1,0:T(8,128)(2,1)S(1)} %bitcast.37, bf16[2048,256]{1,0:T(8,128)(2,1)} %param.14, f32[72,256]{1,0:T(8,128)S(1)} %fusion.25), kind=kOutput, calls=%fused_computation.3 | convolution fusion | flops 151252992 | bytes 2760704 | tf_op jit(solution)/shard_map/dot_general | solution.py:71
  44.0 10.2 %all-gather.4.cloned.1.call-done = bf16[2048,256]{1,0:T(8,128)(2,1)} async-done(((bf16[256,256]{1,0:T(8,128)(2,1)}), bf16[2048,256]{1,0:T(8,128)(2,1)}) %all-gather.4.cloned.1.call-update) | async-done | bytes 1048592 | tf_op jit(solution)/shard_map/all_gather | solution.py:84
  54.2 1.5 fusion.26
  55.7 39.6 %all-gather.6.cloned.1.call-done = bf16[2048,256]{1,0:T(8,128)(2,1)} async-done(((bf16[256,256]{1,0:T(8,128)(2,1)}), bf16[2048,256]{1,0:T(8,128)(2,1)}) %all-gather.6.cloned.1.call-update) | async-done | bytes 1048592 | tf_op jit(solution)/shard_map/all_gather | solution.py:85
  95.3 40.2 %all-gather.8.cloned.1.call-done = bf16[256,2048]{1,0:T(8,128)(2,1)} async-done(((bf16[256,256]{1,0:T(8,128)(2,1)}), bf16[256,2048]{1,0:T(8,128)(2,1)}) %all-gather.8.cloned.1.call-update) | async-done | bytes 1048592 | tf_op jit(solution)/shard_map/all_gather | solution.py:92
  135.4 3.1 %convolution_convert_fusion.1 = bf16[64,2048]{1,0:T(8,128)(2,1)} fusion(bf16[256,2048]{1,0:T(8,128)(2,1)} %all-gather.8.cloned.1.call-done, bf16[64,2048]{1,0:T(8,128)(2,1)S(1)} %copy-done.1, bf16[2048,256]{1,0:T(8,128)(2,1)} %all-gather.6.cloned.1.call-done, f32[64,256]{1,0:T(8,128)S(1)} %fusion.26), kind=kOutput, calls=%fused_computation.2 | convolution fusion | flops 134447104 | bytes 2686976 | tf_op jit(solution)/shard_map/dot_general | solution.py:90
  138.6 1.7 %all_to_all.10 = bf16[1024,8,9]{0,2,1:T(8,128)(2,1)} reshape(bf16[1024,72]{0,1:T(8,128)(2,1)} %reduce-scatter.3.cloned.1.call-done) | data formatting | bytes 294912 | tf_op jit(solution)/shard_map/all_to_all | solution.py:78
  140.2 3.8 %all-to-all-start.1 = ((bf16[1024,8,9]{0,2,1:T(8,128)(2,1)}), bf16[1024,8,9]{0,2,1:T(8,128)(2,1)S(1)}, u32[]{:S(2)}, u32[]{:S(2)}) async-start(bf16[1024,8,9]{0,2,1:T(8,128)(2,1)} %all_to_all.10), calls=%async_computation.2 | async-start | bytes 524288 | tf_op jit(solution)/shard_map/all_to_all | solution.py:78
  144.0 8.2 %all-to-all-done.1 = bf16[1024,8,9]{0,2,1:T(8,128)(2,1)S(1)} async-done(((bf16[1024,8,9]{0,2,1:T(8,128)(2,1)}), bf16[1024,8,9]{0,2,1:T(8,128)(2,1)S(1)}, u32[]{:S(2)}, u32[]{:S(2)}) %all-to-all-start.1) | async-done | bytes 147488 | tf_op jit(solution)/shard_map/all_to_all | solution.py:78
  152.3 0.6 copy-done.5
  153.0 2.0 %fusion.1 = bf16[64,1024]{1,0:T(8,128)(2,1)} fusion(f32[1024,9]{0,1:T(8,128)S(1)} %convert_reduce_fusion, bf16[64,1024]{1,0:T(8,128)(2,1)} %reduce-scatter.5.cloned.1.call-done, f32[1024]{0:T(1024)S(1)} %add_divide_fusion, f32[9]{0:T(128)S(1)} %bitcast.44, s32[9]{0:T(128)S(1)} %bitcast.43), kind=kOutput, calls=%fused_computation.5 | convolution fusion | flops 7341184 | bytes 303176 | tf_op jit(solution)/shard_map/fek,ekt->tf/dot_general | solution.py:82
  (33 shorter events, 0.6 us)
Async XLA Ops:
  7.4 33.8 %copy-start = (bf16[256,2048]{1,0:T(8,128)(2,1)S(1)}, bf16[256,2048]{1,0:T(8,128)(2,1)}, u32[]{:S(2)}) copy-start(bf16[256,2048]{1,0:T(8,128)(2,1)} %param.15) | copy-start | bytes 3145732
  7.4 2.3 %copy-start.1 = (bf16[64,2048]{1,0:T(8,128)(2,1)S(1)}, bf16[64,2048]{1,0:T(8,128)(2,1)}, u32[]{:S(2)}) copy-start(bf16[64,2048]{1,0:T(8,128)(2,1)} %param.10) | copy-start | bytes 786436
  7.4 46.8 %all-gather.4.cloned.1.call-start = ((), (), s32[]{:S(2)}) async-start(), calls=%async_computation.5 | async-start | bytes 1179648 | tf_op jit(solution)/shard_map/all_gather | solution.py:84
  8.1 87.2 %all-gather.6.cloned.1.call-start = ((), (), s32[]{:S(2)}) async-start(), calls=%async_computation.6 | async-start | bytes 1179648 | tf_op jit(solution)/shard_map/all_gather | solution.py:85
  8.8 0.8 copy-start.4
  8.9 126.6 %all-gather.8.cloned.1.call-start = ((), (), s32[]{:S(2)}) async-start(), calls=%async_computation.7 | async-start | bytes 1179648 | tf_op jit(solution)/shard_map/all_gather | solution.py:92
  9.6 129.0 %reduce-scatter.3.cloned.1.call-start = ((), (), s32[]{:S(2)}) async-start(), calls=%async_computation.4 | async-start | bytes 442368 | tf_op jit(solution)/shard_map/reduce_scatter | solution.py:70
  24.5 4.0 %collective-permute-start = (bf16[8,9,1,256]{3,0,2,1:T(8,128)(2,1)S(1)}, bf16[8,9,1,256]{3,0,2,1:T(8,128)(2,1)S(1)}, u32[]{:S(2)}, u32[]{:S(2)}) collective-permute-start(bf16[8,9,1,256]{3,0,2,1:T(8,128)(2,1)S(1)} %bitcast.41), channel_id=1, source_target_pairs={{0,2},{2,0},{4,6},{6,4},{8,10},{10,8},{12,14},{14,12},{1,3},{3,1},... | collective-permute-start | bytes 110600 | tf_op jit(solution)/shard_map/ppermute | solution.py:14
  28.5 4.9 %collective-permute-start.1 = (bf16[8,9,2,256]{3,0,2,1:T(8,128)(2,1)S(1)}, bf16[8,9,2,256]{3,0,2,1:T(8,128)(2,1)S(1)}, u32[]{:S(2)}, u32[]{:S(2)}) collective-permute-start(bf16[8,9,2,256]{3,0,2,1:T(8,128)(2,1)S(1)} %maximum_select_fusion.2), channel_id=1, source_target_pairs={{0,4},{4,0},{2,6},{6,2},{8,12},{12,8},{10,14},{14,10},{1,5},{5,1},... | collective-permute-start | bytes 221192 | tf_op jit(solution)/shard_map/ppermute | solution.py:14
  28.7 12.1 %copy-start.2 = (bf16[2048,256]{1,0:T(8,128)(2,1)S(1)}, bf16[2048,256]{1,0:T(8,128)(2,1)}, u32[]{:S(2)}) copy-start(bf16[2048,256]{1,0:T(8,128)(2,1)} %param.13) | copy-start | bytes 3145732
  33.5 7.2 %collective-permute-start.2 = (bf16[8,9,4,256]{3,0,2,1:T(8,128)(2,1)S(1)}, bf16[8,9,4,256]{3,0,2,1:T(8,128)(2,1)S(1)}, u32[]{:S(2)}, u32[]{:S(2)}) collective-permute-start(bf16[8,9,4,256]{3,0,2,1:T(8,128)(2,1)S(1)} %maximum_select_fusion.1), channel_id=1, source_target_pairs={{0,8},{8,0},{2,10},{10,2},{4,12},{12,4},{6,14},{14,6},{1,9},{9,1},... | collective-permute-start | bytes 442376 | tf_op jit(solution)/shard_map/ppermute | solution.py:14
  43.9 108.4 %reduce-scatter.5.cloned.1.call-start = ((), (), s32[]{:S(2)}) async-start(), calls=%async_computation.8 | async-start | bytes 393216 | tf_op jit(solution)/shard_map/reduce_scatter | solution.py:95
  140.2 3.8 %copy-start.3 = (f32[1024]{0:T(1024)S(1)}, f32[1024]{0:T(1024)}, u32[]{:S(2)}) copy-start(f32[1024]{0:T(1024)} %param.19) | copy-start | bytes 12292
  140.2 12.0 %all-to-all-start.1 = ((bf16[1024,8,9]{0,2,1:T(8,128)(2,1)}), bf16[1024,8,9]{0,2,1:T(8,128)(2,1)S(1)}, u32[]{:S(2)}, u32[]{:S(2)}) async-start(bf16[1024,8,9]{0,2,1:T(8,128)(2,1)} %all_to_all.10), calls=%async_computation.2 | async-start | bytes 524288 | tf_op jit(solution)/shard_map/all_to_all | solution.py:78
  152.3 0.7 copy-start.5
Sparse Core Ops, SparseCore 0:
  10.3 43.8 all-gather.3
  56.3 38.9 all-gather.5
  97.3 38.0 all-gather.7
Sparse Core Ops, SparseCore 1:
  44.0 5.7 reduce-scatter.2
  138.6 6.7 reduce-scatter.4
where the time goes:
time: 163 us; the launch traced here: 162 us
  waiting for transfers between devices  115 us (71%)
  between operations  14.7 us (9%)
  blocking collectives  14.1 us (9%)
  matrix products  9.66 us (6%)
  starting transfers between devices  4.97 us (3%)
  local copies, waits for them, and re-layouts  3.09 us (2%)
    all_gather x1, waiting for transfers between devices, local(): lax.all_gather(dense_down, 'ep', axis=1, tiled=True)  40.2 us
    all_gather x1, waiting for transfers between devices, local(): lax.all_gather(dense_up, 'ep', axis=0, tiled=True)  39.6 us
    ppermute x3, waiting for transfers between devices, swapped(): return lax.ppermute(block, axis, route)  15.1 us
    all_to_all x1, blocking collectives, local(): lax.all_to_all(split_rows, 'ep', split_axis=0, concat_axis=0, tiled=True)  14.1 us
    all_gather x1, waiting for transfers between devices, local(): lax.all_gather(dense_gate, 'ep', axis=0, tiled=True)  10.2 us
    all_to_all x1, waiting for transfers between devices, local(): lax.all_to_all(member_sums, 'ep', split_axis=1, concat_axis=1, tiled=True)  8.21 us
    all_to_all x1, starting transfers between devices, local(): lax.all_to_all(member_sums, 'ep', split_axis=1, concat_axis=1, tiled=True)  3.76 us
  transfers between devices with their start and end apart: 9, of which 7 were waited for; matrix products, arithmetic and copies ran while one was open for 5% of the time, Pallas kernels for 0%

commit v1 on v0

--- a/solution.py
+++ b/solution.py
@@ -1,7 +1,13 @@
+import functools
+
 import jax
 import jax.numpy as jnp
 from jax import lax
+from jax.experimental import pallas as pl
+from jax.experimental.pallas import tpu as pltpu
 from jax.sharding import PartitionSpec as P
+
+MESH = pl.DeviceIdType.MESH
 
 
 def swapped(block, axis, apart):
@@ -26,7 +32,374 @@
     return jnp.where(upper, jnp.concatenate([theirs, mine], 2), jnp.concatenate([mine, theirs], 2))
 
 
-def local(
+def fused_kernel(
+    n,
+    tok_ref,
+    chosen_ref,
+    route_ref,
+    eg_hbm,
+    eu_hbm,
+    ed_hbm,
+    dg_ref,
+    du_ref,
+    dd_ref,
+    bg_ref,
+    out_ref,
+    eg,
+    eu,
+    ed,
+    weights,
+    tok_all,
+    table,
+    rows_all,
+    part_send,
+    part_recv,
+    hid_all,
+    down_send,
+    down_recv,
+    half_send,
+    half_recv,
+    ret_send,
+    ret_recv,
+    local_sem,
+    w_send,
+    w_recv,
+    t_send,
+    t_recv,
+    tf_send,
+    tf_recv,
+    r_send,
+    r_recv,
+    rf_send,
+    rf_recv,
+    p_send,
+    p_recv,
+    h_send,
+    h_recv,
+    d_send,
+    d_recv,
+    s_send,
+    s_recv,
+    m_send,
+    m_recv,
+):
+    f32, bf16 = jnp.float32, jnp.bfloat16
+    ep, tp = lax.axis_index("ep"), lax.axis_index("tp")
+    sib = 1 - tp
+    nz = n // 2
+    x, z = lax.rem(ep, 2), lax.div(ep, 2)
+    toks, width = tok_ref.shape
+    feat = width // nz
+    halfw = width // 2
+    spad = rows_all.shape[2]
+    hidden = dg_ref.shape[1]
+    pos_count = nz // 2
+
+    def line(d):
+        return lax.rem(z + d + nz, nz) * 2 + x
+
+    def ring(d):
+        return lax.rem(ep + d + n, n)
+
+    sends = []
+
+    def remote(src, dst, ssem, rsem, to_ep, to_tp, go=True):
+        copy = pltpu.make_async_remote_copy(
+            src_ref=src,
+            dst_ref=dst,
+            send_sem=ssem,
+            recv_sem=rsem,
+            device_id={"ep": to_ep, "tp": to_tp},
+            device_id_type=MESH,
+        )
+        if go:
+            copy.start()
+            sends.append(copy)
+        return copy
+
+    loads = []
+    for i, (src, dst) in enumerate(((eg_hbm, eg), (eu_hbm, eu), (ed_hbm, ed))):
+        load = pltpu.make_async_copy(src, dst, local_sem.at[i])
+        load.start()
+        loads.append(load)
+
+    barrier = pltpu.get_barrier_semaphore()
+    for d in range(1, n):
+        pl.semaphore_signal(
+            barrier, inc=1, device_id={"ep": ring(d), "tp": tp}, device_id_type=MESH
+        )
+    for d in range(nz):
+        pl.semaphore_signal(
+            barrier, inc=1, device_id={"ep": line(d), "tp": sib}, device_id_type=MESH
+        )
+
+    table[...] = jnp.full(table.shape, -1.0, f32)
+    slots = chosen_ref.shape[2]
+    table[0:1, 0:slots] = chosen_ref[0].astype(f32)
+    table[8:9, 0:slots] = route_ref[0]
+    token_id = lax.broadcasted_iota(jnp.int32, (toks, table.shape[1]), 0).astype(f32)
+    match = token_id == table[0:1, :]
+    onehot = jnp.where(match, 1.0, 0.0).astype(f32)
+    pick = onehot.T[:spad].astype(bf16)
+    picked = jnp.dot(pick, tok_ref[...], preferred_element_type=f32).astype(bf16)
+    rows_all[0, 0] = picked[:, :halfw]
+    rows_all[1, 0] = picked[:, halfw:]
+
+    pl.semaphore_wait(barrier, n - 1 + nz)
+
+    th = toks // 2
+    mine = pl.ds(pl.multiple_of(tp * th, th), th)
+    theirs = pl.ds(pl.multiple_of(sib * th, th), th)
+    tcopies = []
+    for d in range(1, nz):
+        cols = pl.ds(pl.multiple_of(lax.rem(z + d, nz) * feat, feat), feat)
+        tcopies.append(
+            remote(
+                tok_ref.at[mine, cols],
+                tok_all.at[d, mine],
+                t_send.at[d],
+                t_recv.at[d],
+                line(d),
+                tp,
+            )
+        )
+    pair = ep + 1 - 2 * x
+    wcopies = []
+    for i, src in enumerate((dg_ref, du_ref, dd_ref)):
+        wcopies.append(
+            remote(src, weights.at[i, x], w_send.at[i], w_recv.at[i], pair, tp)
+        )
+    rcopies = []
+    for d in range(1, n):
+        rcopies.append(
+            remote(
+                rows_all.at[tp, 0], rows_all.at[tp, d], r_send.at[d], r_recv.at[d], ring(d), tp
+            )
+        )
+
+    own_cols = pl.ds(pl.multiple_of(z * feat, feat), feat)
+    tok_all[0] = tok_ref[:, own_cols]
+    for i, src in enumerate((dg_ref, du_ref, dd_ref)):
+        weights[i, x] = src[...]
+
+    for d in range(1, nz):
+        tcopies[d - 1].wait_recv()
+        remote(
+            tok_all.at[d, mine], tok_all.at[d, mine], tf_send.at[d], tf_recv.at[d], ep, sib
+        )
+    wait_at = lambda dst, ssem, rsem: remote(dst, dst, ssem, rsem, ep, sib, go=False).wait_recv()
+
+    def wait_on(ssem, rsem, dst):
+        wait_at(dst, ssem, rsem)
+
+    for i in range(2):
+        remote(dg_ref, weights.at[i, 1 - x], w_send.at[i], w_recv.at[i], pair, tp, go=False).wait_recv()
+    for d in range(1, nz):
+        wait_on(tf_send.at[d], tf_recv.at[d], tok_all.at[d, theirs])
+    toks_in = tok_all[...].reshape(nz * toks, feat)
+    fh = feat // 2
+    sums = []
+    for i in range(2):
+        total = jnp.dot(toks_in[:, :fh], weights[i, 0], preferred_element_type=f32) + jnp.dot(
+            toks_in[:, fh:], weights[i, 1], preferred_element_type=f32
+        )
+        sums.append(total[:toks])
+        for d in range(1, nz):
+            part_send[d - 1, i] = total[d * toks : (d + 1) * toks].astype(bf16)
+    pcopies = []
+    for d in range(1, nz):
+        pcopies.append(
+            remote(
+                part_send.at[d - 1], part_recv.at[d - 1], p_send.at[d], p_recv.at[d], line(-d), tp
+            )
+        )
+
+    for d in range(1, n):
+        rcopies[d - 1].wait_recv()
+        remote(
+            rows_all.at[tp, d], rows_all.at[tp, d], rf_send.at[d], rf_recv.at[d], ep, sib
+        )
+    for load in loads[:2]:
+        load.wait()
+    for d in range(1, n):
+        wait_on(rf_send.at[d], rf_recv.at[d], rows_all.at[sib, d])
+    low = rows_all[0].reshape(n * spad, halfw)
+    high = rows_all[1].reshape(n * spad, halfw)
+
+    def project(w):
+        return jnp.dot(low, w[:halfw], preferred_element_type=f32) + jnp.dot(
+            high, w[halfw:], preferred_element_type=f32
+        )
+
+    gate = project(eg)
+    up = project(eu)
+    act = (gate / (1.0 + jnp.exp(-gate)) * up).astype(bf16)
+    loads[2].wait()
+    off = pl.ds(pl.multiple_of(sib * halfw, halfw), halfw)
+    keep = pl.ds(pl.multiple_of(tp * halfw, halfw), halfw)
+    half_send[...] = jnp.dot(act, ed[:, off], preferred_element_type=f32).astype(bf16)
+    scopy = remote(half_send, half_recv, s_send, s_recv, ep, sib)
+
+    for d in range(1, nz):
+        pcopies[d - 1].wait_recv()
+        sums = [sums[i] + part_recv[d - 1, i].astype(f32) for i in range(2)]
+    dense_hidden = (sums[0] / (1.0 + jnp.exp(-sums[0])) * sums[1]).astype(bf16)
+    hid_all[0] = dense_hidden
+    hcopies = []
+    for d in range(1, nz):
+        hcopies.append(
+            remote(hid_all.at[0], hid_all.at[d], h_send.at[d], h_recv.at[d], line(d), tp)
+        )
+
+    own_half = jnp.dot(act, ed[:, keep], preferred_element_type=f32).astype(bf16)
+    scopy.wait_recv()
+    member = (own_half.astype(f32) + half_recv[...].astype(f32)).astype(bf16)
+    ret_send[...] = member.reshape(n, spad, halfw)
+    mcopies = []
+    for d in range(1, n):
+        mcopies.append(
+            remote(ret_send.at[d], ret_recv.at[d - 1], m_send.at[d], m_recv.at[d], ring(-d), tp)
+        )
+
+    remote(dd_ref, weights.at[2, 1 - x], w_send.at[2], w_recv.at[2], pair, tp, go=False).wait_recv()
+    for d in range(1, nz):
+        hcopies[d - 1].wait_recv()
+    owner = lax.div(z, pos_count)
+    place = lax.rem(z, pos_count)
+    hid_in = hid_all[...].reshape(nz * toks, hidden)
+    for i in range(2):
+        part = jnp.dot(hid_in, weights[2, i], preferred_element_type=f32).astype(bf16)
+        down_send[:, :, i * fh : (i + 1) * fh] = part.reshape(nz, toks, fh)
+    for d in range(1, nz):
+        remote(
+            down_send.at[d],
+            down_recv.at[place, tp],
+            d_send.at[d],
+            d_recv.at[place, tp],
+            line(-d),
+            owner,
+        )
+
+    def sibling_copy():
+        return remote(
+            down_send.at[0],
+            down_recv.at[place, tp],
+            d_send.at[0],
+            d_recv.at[place, tp],
+            ep,
+            sib,
+            go=False,
+        )
+
+    @pl.when(owner != tp)
+    def _():
+        sibling_copy().start()
+
+    @pl.when(owner == tp)
+    def _():
+        down_recv[place, tp] = down_send[0]
+
+    total = ret_send[0].astype(f32)
+    for d in range(1, n):
+        mcopies[d - 1].wait_recv()
+        total = total + ret_recv[d - 1].astype(f32)
+    spread = jnp.where(match, table[8:9, :], 0.0)[:, :spad]
+    combined = jnp.dot(
+        spread, total, preferred_element_type=f32, precision=lax.Precision.HIGHEST
+    )
+    for p in range(pos_count):
+        for t in range(2):
+
+            @pl.when(jnp.logical_or(tp * pos_count + p != z, tp != t))
+            def _():
+                wait_on(d_send.at[0], d_recv.at[p, t], down_recv.at[p, t])
+
+        cols = slice(p * feat, (p + 1) * feat)
+        dense = down_recv[p, 0].astype(f32) + down_recv[p, 1].astype(f32)
+        scale = 1.0 / (1.0 + jnp.exp(-bg_ref[:, cols]))
+        out_ref[:, cols] = (combined[:, cols] + scale * dense).astype(bf16)
+
+    for copy in sends:
+        copy.wait_send()
+
+    @pl.when(owner != tp)
+    def _():
+        sibling_copy().wait_send()
+
+
+def fused_local(n, *args):
+    tokens, chosen, dense_gate, branch_gate = args[0], args[1], args[6], args[9]
+    toks, width = tokens.shape
+    nz = n // 2
+    feat = width // nz
+    spad = -(-chosen.shape[2] // 16) * 16
+    hid = dense_gate.shape[1]
+    units = args[3].shape[1]
+    bf16 = jnp.bfloat16
+    vmem = pl.BlockSpec(memory_space=pltpu.VMEM)
+    hbm = pl.BlockSpec(memory_space=pl.ANY)
+    dma = pltpu.SemaphoreType.DMA
+    scratch = [
+        pltpu.VMEM((width, units), bf16),
+        pltpu.VMEM((width, units), bf16),
+        pltpu.VMEM((units, width), bf16),
+        pltpu.VMEM((3, 2) + dense_gate.shape, bf16),
+        pltpu.VMEM((nz, toks, feat), bf16),
+        pltpu.VMEM((16, 128), jnp.float32),
+        pltpu.VMEM((2, n, spad, width // 2), bf16),
+        pltpu.VMEM((nz - 1, 2, toks, hid), bf16),
+        pltpu.VMEM((nz - 1, 2, toks, hid), bf16),
+        pltpu.VMEM((nz, toks, hid), bf16),
+        pltpu.VMEM((nz, toks, feat), bf16),
+        pltpu.VMEM((nz // 2, 2, toks, feat), bf16),
+        pltpu.VMEM((n * spad, width // 2), bf16),
+        pltpu.VMEM((n * spad, width // 2), bf16),
+        pltpu.VMEM((n, spad, width // 2), bf16),
+        pltpu.VMEM((n - 1, spad, width // 2), bf16),
+        dma((3,)),
+        dma((3,)),
+        dma((3,)),
+        dma((nz,)),
+        dma((nz,)),
+        dma((nz,)),
+        dma((nz,)),
+        dma((n,)),
+        dma((n,)),
+        dma((n,)),
+        dma((n,)),
+        dma((nz,)),
+        dma((nz,)),
+        dma((nz,)),
+        dma((nz,)),
+        dma((nz,)),
+        dma((nz // 2, 2)),
+        dma,
+        dma,
+        dma((n,)),
+        dma((n,)),
+    ]
+    return pl.pallas_call(
+        functools.partial(fused_kernel, n),
+        out_shape=jax.ShapeDtypeStruct((toks, width // 2), bf16),
+        in_specs=[vmem] * 3 + [hbm] * 3 + [vmem] * 4,
+        out_specs=vmem,
+        scratch_shapes=scratch,
+        compiler_params=pltpu.CompilerParams(collective_id=0, has_side_effects=True),
+    )(*args[:9], branch_gate.reshape(1, -1))
+
+
+def local(*args):
+    n = lax.axis_size("ep")
+    tokens, chosen, dense_gate = args[0], args[1], args[6]
+    width = tokens.shape[1]
+    square = dense_gate.shape[0] == dense_gate.shape[1] == args[8].shape[1]
+    fits = chosen.shape[0] == 1 and n % 4 == 0 and square
+    fits = fits and (width // n) % 128 == 0 and tokens.shape[0] % 32 == 0
+    fits = fits and chosen.shape[2] <= 128 and lax.axis_size("tp") == 2
+    return fused_local(n, *args) if fits else plain_local(*args)
+
+
+def plain_local(
     tokens,
     chosen,
     route_weight,

time: 163 us -> 40.7 us (0.25)
  the two profiles are of different devices: /device:TPU:0 before, /device:TPU:1 now
where the time goes in v1:
time: 40.7 us; the launch traced here: 40.6 us
  Pallas kernels  39 us (96%)
  local copies, waits for them, and re-layouts  1.57 us (4%)
    pallas_call x1, Pallas kernels, fused_local(): pl.pallas_call(functools.partial(fused_kernel, n), out_shape=jax.ShapeDty...  39 us
    unnamed x1, local copies, waits for them, and re-layouts  1.57 us

profile of v1, /device:TPU:1, one launch (start us, length us, event | category | flops | bytes accessed | tf_op | source)
XLA Modules:
  0.0 40.6 jit_solution(16450543576382768319)
XLA Ops:
  0.0 39.0 %shard_map.100 = bf16[64,1024]{1,0:T(8,128)(2,1)} custom-call(bf16[64,2048]{1,0:T(8,128)(2,1)} %tok_ref.1, s32[1,1,9]{2,1,0:T(1,128)} %chosen_ref.1, f32[1,1,9]{2,1,0:T(1,128)} %route_ref.1, bf16[2048,256]{1,0:T(8,128)(2,1)} %eg_hbm.1, bf16[2048,256]{1,0:T(8,128)(2,1)} %eu_hbm.1, bf16[256,2048]{1,0:T(8,128)(2,1)} %ed_hbm.1, bf16[256,256]{1,0:T(8,128)(2,1)} %dg_ref.1, ...), custom_call_target="tpu_custom_call" | custom-call | tf_op jit(solution)/shard_map/pallas_call | solution.py:381
  39.0 1.6 %copy.12 = bf16[64,1024]{1,0:T(8,128)(2,1)} copy(bf16[64,1024]{1,0:T(8,128)(2,1)} %shard_map.100) | data formatting | bytes 262144

commit v2 on v1

--- a/solution.py
+++ b/solution.py
@@ -52,6 +52,8 @@
     tok_all,
     table,
     rows_all,
+    ext_all,
+    ext_wide,
     part_send,
     part_recv,
     hid_all,
@@ -61,6 +63,8 @@
     half_recv,
     ret_send,
     ret_recv,
+    rex_send,
+    rex_recv,
     local_sem,
     w_send,
     w_recv,
@@ -91,7 +95,8 @@
     toks, width = tok_ref.shape
     feat = width // nz
     halfw = width // 2
-    spad = rows_all.shape[2]
+    base = rows_all.shape[2]
+    chunks = halfw // 128
     hidden = dg_ref.shape[1]
     pos_count = nz // 2
 
@@ -135,15 +140,23 @@
 
     table[...] = jnp.full(table.shape, -1.0, f32)
     slots = chosen_ref.shape[2]
+    extra = slots - base
+    spad = -(-slots // 16) * 16
     table[0:1, 0:slots] = chosen_ref[0].astype(f32)
     table[8:9, 0:slots] = route_ref[0]
     token_id = lax.broadcasted_iota(jnp.int32, (toks, table.shape[1]), 0).astype(f32)
     match = token_id == table[0:1, :]
     onehot = jnp.where(match, 1.0, 0.0).astype(f32)
     pick = onehot.T[:spad].astype(bf16)
-    picked = jnp.dot(pick, tok_ref[...], preferred_element_type=f32).astype(bf16)
-    rows_all[0, 0] = picked[:, :halfw]
-    rows_all[1, 0] = picked[:, halfw:]
+    picked = jnp.dot(pick, tok_ref[...], preferred_element_type=f32)
+    for h in range(2):
+        rows_all[h, 0] = picked[:base, h * halfw : (h + 1) * halfw].astype(bf16)
+        pieces = [
+            picked[base + k : base + k + 1, h * halfw + c * 128 : h * halfw + (c + 1) * 128]
+            for k in range(extra)
+            for c in range(chunks)
+        ]
+        ext_all[h, 0] = jnp.concatenate(pieces, 0).astype(bf16)
 
     pl.semaphore_wait(barrier, n - 1 + nz)
 
@@ -169,11 +182,21 @@
         wcopies.append(
             remote(src, weights.at[i, x], w_send.at[i], w_recv.at[i], pair, tp)
         )
-    rcopies = []
+    rcopies, ecopies = [], []
     for d in range(1, n):
         rcopies.append(
             remote(
                 rows_all.at[tp, 0], rows_all.at[tp, d], r_send.at[d], r_recv.at[d], ring(d), tp
+            )
+        )
+        ecopies.append(
+            remote(
+                ext_all.at[tp, 0],
+                ext_all.at[tp, d],
+                r_send.at[n + d],
+                r_recv.at[n + d],
+                ring(d),
+                tp,
             )
         )
 
@@ -219,12 +242,29 @@
         remote(
             rows_all.at[tp, d], rows_all.at[tp, d], rf_send.at[d], rf_recv.at[d], ep, sib
         )
+        ecopies[d - 1].wait_recv()
+        remote(
+            ext_all.at[tp, d], ext_all.at[tp, d], rf_send.at[n + d], rf_recv.at[n + d], ep, sib
+        )
     for load in loads[:2]:
         load.wait()
     for d in range(1, n):
         wait_on(rf_send.at[d], rf_recv.at[d], rows_all.at[sib, d])
-    low = rows_all[0].reshape(n * spad, halfw)
-    high = rows_all[1].reshape(n * spad, halfw)
+        wait_on(rf_send.at[n + d], rf_recv.at[n + d], ext_all.at[sib, d])
+    ext_wide[...] = ext_all[...].astype(f32)
+    every = half_send.shape[0]
+
+    def stacked(h):
+        parts = [rows_all[h].astype(f32).reshape(n * base, halfw)]
+        for k in range(extra):
+            parts.append(
+                jnp.concatenate([ext_wide[h, :, k * chunks + c, :] for c in range(chunks)], 1)
+            )
+        if every > n * slots:
+            parts.append(jnp.zeros((every - n * slots, halfw), f32))
+        return jnp.concatenate(parts, 0).astype(bf16)
+
+    low, high = stacked(0), stacked(1)
 
     def project(w):
         return jnp.dot(low, w[:halfw], preferred_element_type=f32) + jnp.dot(
@@ -253,12 +293,22 @@
 
     own_half = jnp.dot(act, ed[:, keep], preferred_element_type=f32).astype(bf16)
     scopy.wait_recv()
-    member = (own_half.astype(f32) + half_recv[...].astype(f32)).astype(bf16)
-    ret_send[...] = member.reshape(n, spad, halfw)
-    mcopies = []
+    member = own_half.astype(f32) + half_recv[...].astype(f32)
+    ret_send[...] = member[: n * base].reshape(n, base, halfw).astype(bf16)
+    for k in range(extra):
+        first = n * (base + k)
+        for c in range(chunks):
+            ext_wide[0, :, k * chunks + c, :] = member[first : first + n, c * 128 : (c + 1) * 128]
+    rex_send[...] = ext_wide[0].astype(bf16)
+    mcopies, xcopies = [], []
     for d in range(1, n):
         mcopies.append(
             remote(ret_send.at[d], ret_recv.at[d - 1], m_send.at[d], m_recv.at[d], ring(-d), tp)
+        )
+        xcopies.append(
+            remote(
+                rex_send.at[d], rex_recv.at[d - 1], m_send.at[n + d], m_recv.at[n + d], ring(-d), tp
+            )
         )
 
     remote(dd_ref, weights.at[2, 1 - x], w_send.at[2], w_recv.at[2], pair, tp, go=False).wait_recv()
@@ -300,9 +350,21 @@
         down_recv[place, tp] = down_send[0]
 
     total = ret_send[0].astype(f32)
+    ext_total = rex_send[0].astype(f32)
     for d in range(1, n):
         mcopies[d - 1].wait_recv()
+        xcopies[d - 1].wait_recv()
         total = total + ret_recv[d - 1].astype(f32)
+        ext_total = ext_total + rex_recv[d - 1].astype(f32)
+    if spad > base:
+        row_id = lax.broadcasted_iota(jnp.int32, (spad - base, halfw), 0)
+        tail = jnp.zeros((spad - base, halfw), f32)
+        for k in range(extra):
+            row = jnp.concatenate(
+                [ext_total[k * chunks + c : k * chunks + c + 1, :] for c in range(chunks)], 1
+            )
+            tail = jnp.where(row_id == k, row, tail)
+        total = jnp.concatenate([total, tail], 0)
     spread = jnp.where(match, table[8:9, :], 0.0)[:, :spad]
     combined = jnp.dot(
         spread, total, preferred_element_type=f32, precision=lax.Precision.HIGHEST
@@ -332,7 +394,10 @@
     toks, width = tokens.shape
     nz = n // 2
     feat = width // nz
-    spad = -(-chosen.shape[2] // 16) * 16
+    slots = chosen.shape[2]
+    base = slots // 8 * 8
+    lines = (slots - base) * (width // 256)
+    every = -(-n * slots // 16) * 16
     hid = dense_gate.shape[1]
     units = args[3].shape[1]
     bf16 = jnp.bfloat16
@@ -346,16 +411,20 @@
         pltpu.VMEM((3, 2) + dense_gate.shape, bf16),
         pltpu.VMEM((nz, toks, feat), bf16),
         pltpu.VMEM((16, 128), jnp.float32),
-        pltpu.VMEM((2, n, spad, width // 2), bf16),
+        pltpu.VMEM((2, n, base, width // 2), bf16),
+        pltpu.VMEM((2, n, lines, 128), bf16),
+        pltpu.VMEM((2, n, lines, 128), jnp.float32),
         pltpu.VMEM((nz - 1, 2, toks, hid), bf16),
         pltpu.VMEM((nz - 1, 2, toks, hid), bf16),
         pltpu.VMEM((nz, toks, hid), bf16),
         pltpu.VMEM((nz, toks, feat), bf16),
         pltpu.VMEM((nz // 2, 2, toks, feat), bf16),
-        pltpu.VMEM((n * spad, width // 2), bf16),
-        pltpu.VMEM((n * spad, width // 2), bf16),
-        pltpu.VMEM((n, spad, width // 2), bf16),
-        pltpu.VMEM((n - 1, spad, width // 2), bf16),
+        pltpu.VMEM((every, width // 2), bf16),
+        pltpu.VMEM((every, width // 2), bf16),
+        pltpu.VMEM((n, base, width // 2), bf16),
+        pltpu.VMEM((n - 1, base, width // 2), bf16),
+        pltpu.VMEM((n, lines, 128), bf16),
+        pltpu.VMEM((n - 1, lines, 128), bf16),
         dma((3,)),
         dma((3,)),
         dma((3,)),
@@ -363,10 +432,10 @@
         dma((nz,)),
         dma((nz,)),
         dma((nz,)),
-        dma((n,)),
-        dma((n,)),
-        dma((n,)),
-        dma((n,)),
+        dma((2 * n,)),
+        dma((2 * n,)),
+        dma((2 * n,)),
+        dma((2 * n,)),
         dma((nz,)),
         dma((nz,)),
         dma((nz,)),
@@ -375,8 +444,8 @@
         dma((nz // 2, 2)),
         dma,
         dma,
-        dma((n,)),
-        dma((n,)),
+        dma((2 * n,)),
+        dma((2 * n,)),
     ]
     return pl.pallas_call(
         functools.partial(fused_kernel, n),
@@ -395,6 +464,7 @@
     square = dense_gate.shape[0] == dense_gate.shape[1] == args[8].shape[1]
     fits = chosen.shape[0] == 1 and n % 4 == 0 and square
     fits = fits and (width // n) % 128 == 0 and tokens.shape[0] % 32 == 0
+    fits = fits and chosen.shape[2] > 8 and chosen.shape[2] % 8 != 0 and width % 2048 == 0
     fits = fits and chosen.shape[2] <= 128 and lax.axis_size("tp") == 2
     return fused_local(n, *args) if fits else plain_local(*args)
 

time: 40.7 us -> 37.4 us (0.919)
  Pallas kernels: 39 us -> 35.7 us
    pallas_call x1, Pallas kernels: 39 us -> 35.7 us  [fused_local(): pl.pallas_call(functools.partial(fused_kernel, n), out_shape=jax.ShapeDty...]
where the time goes in v2:
time: 37.4 us; the launch traced here: 37.3 us
  Pallas kernels  35.7 us (95%)
  local copies, waits for them, and re-layouts  1.57 us (4%)
    pallas_call x1, Pallas kernels, fused_local(): pl.pallas_call(functools.partial(fused_kernel, n), out_shape=jax.ShapeDty...  35.7 us
    unnamed x1, local copies, waits for them, and re-layouts  1.57 us

profile of v2, /device:TPU:1, one launch (start us, length us, event | category | flops | bytes accessed | tf_op | source)
XLA Modules:
  0.0 37.3 jit_solution(15569508647347048119)
XLA Ops:
  0.0 35.7 %shard_map.100 = bf16[64,1024]{1,0:T(8,128)(2,1)} custom-call(bf16[64,2048]{1,0:T(8,128)(2,1)} %tok_ref.1, s32[1,1,9]{2,1,0:T(1,128)} %chosen_ref.1, f32[1,1,9]{2,1,0:T(1,128)} %route_ref.1, bf16[2048,256]{1,0:T(8,128)(2,1)} %eg_hbm.1, bf16[2048,256]{1,0:T(8,128)(2,1)} %eu_hbm.1, bf16[256,2048]{1,0:T(8,128)(2,1)} %ed_hbm.1, bf16[256,256]{1,0:T(8,128)(2,1)} %dg_ref.1, ...), custom_call_target="tpu_custom_call" | custom-call | tf_op jit(solution)/shard_map/pallas_call | solution.py:450
  35.7 1.6 %copy.12 = bf16[64,1024]{1,0:T(8,128)(2,1)} copy(bf16[64,1024]{1,0:T(8,128)(2,1)} %shard_map.100) | data formatting | bytes 262144

commit v3 on v2

--- a/solution.py
+++ b/solution.py
@@ -34,17 +34,18 @@
 
 def fused_kernel(
     n,
-    tok_ref,
+    tok_hbm,
     chosen_ref,
     route_ref,
     eg_hbm,
     eu_hbm,
     ed_hbm,
-    dg_ref,
-    du_ref,
-    dd_ref,
+    dg_hbm,
+    du_hbm,
+    dd_hbm,
     bg_ref,
     out_ref,
+    tok_ref,
     eg,
     eu,
     ed,
@@ -59,6 +60,8 @@
     hid_all,
     down_send,
     down_recv,
+    pre_send,
+    pre_recv,
     half_send,
     half_recv,
     ret_send,
@@ -84,6 +87,8 @@
     d_recv,
     s_send,
     s_recv,
+    q_send,
+    q_recv,
     m_send,
     m_recv,
 ):
@@ -97,7 +102,7 @@
     halfw = width // 2
     base = rows_all.shape[2]
     chunks = halfw // 128
-    hidden = dg_ref.shape[1]
+    hidden = weights.shape[3]
     pos_count = nz // 2
 
     def line(d):
@@ -123,10 +128,13 @@
         return copy
 
     loads = []
-    for i, (src, dst) in enumerate(((eg_hbm, eg), (eu_hbm, eu), (ed_hbm, ed))):
+    plan = ((eg_hbm, eg), (eu_hbm, eu), (ed_hbm, ed), (tok_hbm, tok_ref))
+    plan += tuple((w, weights.at[i, x]) for i, w in enumerate((dg_hbm, du_hbm, dd_hbm)))
+    for i, (src, dst) in enumerate(plan[3:] + plan[:3]):
         load = pltpu.make_async_copy(src, dst, local_sem.at[i])
         load.start()
         loads.append(load)
+    early, loads = loads[:4], loads[4:]
 
     barrier = pltpu.get_barrier_semaphore()
     for d in range(1, n):
@@ -147,6 +155,7 @@
     token_id = lax.broadcasted_iota(jnp.int32, (toks, table.shape[1]), 0).astype(f32)
     match = token_id == table[0:1, :]
     onehot = jnp.where(match, 1.0, 0.0).astype(f32)
+    early[0].wait()
     pick = onehot.T[:spad].astype(bf16)
     picked = jnp.dot(pick, tok_ref[...], preferred_element_type=f32)
     for h in range(2):
@@ -177,11 +186,10 @@
             )
         )
     pair = ep + 1 - 2 * x
-    wcopies = []
-    for i, src in enumerate((dg_ref, du_ref, dd_ref)):
-        wcopies.append(
-            remote(src, weights.at[i, x], w_send.at[i], w_recv.at[i], pair, tp)
-        )
+    for i in range(3):
+        early[1 + i].wait()
+        own = weights.at[i, x]
+        remote(own, own, w_send.at[i], w_recv.at[i], pair, tp)
     rcopies, ecopies = [], []
     for d in range(1, n):
         rcopies.append(
@@ -202,8 +210,6 @@
 
     own_cols = pl.ds(pl.multiple_of(z * feat, feat), feat)
     tok_all[0] = tok_ref[:, own_cols]
-    for i, src in enumerate((dg_ref, du_ref, dd_ref)):
-        weights[i, x] = src[...]
 
     for d in range(1, nz):
         tcopies[d - 1].wait_recv()
@@ -216,7 +222,7 @@
         wait_at(dst, ssem, rsem)
 
     for i in range(2):
-        remote(dg_ref, weights.at[i, 1 - x], w_send.at[i], w_recv.at[i], pair, tp, go=False).wait_recv()
+        remote(weights.at[i, x], weights.at[i, 1 - x], w_send.at[i], w_recv.at[i], pair, tp, go=False).wait_recv()
     for d in range(1, nz):
         wait_on(tf_send.at[d], tf_recv.at[d], tok_all.at[d, theirs])
     toks_in = tok_all[...].reshape(nz * toks, feat)
@@ -311,15 +317,19 @@
             )
         )
 
-    remote(dd_ref, weights.at[2, 1 - x], w_send.at[2], w_recv.at[2], pair, tp, go=False).wait_recv()
+    remote(weights.at[2, x], weights.at[2, 1 - x], w_send.at[2], w_recv.at[2], pair, tp, go=False).wait_recv()
     for d in range(1, nz):
         hcopies[d - 1].wait_recv()
     owner = lax.div(z, pos_count)
     place = lax.rem(z, pos_count)
     hid_in = hid_all[...].reshape(nz * toks, hidden)
-    for i in range(2):
-        part = jnp.dot(hid_in, weights[2, i], preferred_element_type=f32).astype(bf16)
-        down_send[:, :, i * fh : (i + 1) * fh] = part.reshape(nz, toks, fh)
+    away = jnp.dot(hid_in, weights[2, sib], preferred_element_type=f32)
+    pre_send[...] = away.astype(bf16)
+    qcopy = remote(pre_send, pre_recv, q_send, q_recv, ep, sib)
+    part = jnp.dot(hid_in, weights[2, tp], preferred_element_type=f32)
+    qcopy.wait_recv()
+    part = part + pre_recv[...].astype(f32)
+    down_send[...] = part.astype(bf16).reshape(nz, toks, fh)
     for d in range(1, nz):
         remote(
             down_send.at[d],
@@ -376,10 +386,11 @@
             def _():
                 wait_on(d_send.at[0], d_recv.at[p, t], down_recv.at[p, t])
 
-        cols = slice(p * feat, (p + 1) * feat)
-        dense = down_recv[p, 0].astype(f32) + down_recv[p, 1].astype(f32)
-        scale = 1.0 / (1.0 + jnp.exp(-bg_ref[:, cols]))
-        out_ref[:, cols] = (combined[:, cols] + scale * dense).astype(bf16)
+        for t in range(2):
+            cols = slice(p * feat + t * fh, p * feat + (t + 1) * fh)
+            dense = down_recv[p, t].astype(f32)
+            scale = 1.0 / (1.0 + jnp.exp(-bg_ref[:, cols]))
+            out_ref[:, cols] = (combined[:, cols] + scale * dense).astype(bf16)
 
     for copy in sends:
         copy.wait_send()
@@ -405,6 +416,7 @@
     hbm = pl.BlockSpec(memory_space=pl.ANY)
     dma = pltpu.SemaphoreType.DMA
     scratch = [
+        pltpu.VMEM((toks, width), bf16),
         pltpu.VMEM((width, units), bf16),
         pltpu.VMEM((width, units), bf16),
         pltpu.VMEM((units, width), bf16),
@@ -417,15 +429,17 @@
         pltpu.VMEM((nz - 1, 2, toks, hid), bf16),
         pltpu.VMEM((nz - 1, 2, toks, hid), bf16),
         pltpu.VMEM((nz, toks, hid), bf16),
-        pltpu.VMEM((nz, toks, feat), bf16),
-        pltpu.VMEM((nz // 2, 2, toks, feat), bf16),
+        pltpu.VMEM((nz, toks, feat // 2), bf16),
+        pltpu.VMEM((nz // 2, 2, toks, feat // 2), bf16),
+        pltpu.VMEM((nz * toks, feat // 2), bf16),
+        pltpu.VMEM((nz * toks, feat // 2), bf16),
         pltpu.VMEM((every, width // 2), bf16),
         pltpu.VMEM((every, width // 2), bf16),
         pltpu.VMEM((n, base, width // 2), bf16),
         pltpu.VMEM((n - 1, base, width // 2), bf16),
         pltpu.VMEM((n, lines, 128), bf16),
         pltpu.VMEM((n - 1, lines, 128), bf16),
-        dma((3,)),
+        dma((7,)),
         dma((3,)),
         dma((3,)),
         dma((nz,)),
@@ -442,6 +456,8 @@
         dma((nz,)),
         dma((nz,)),
         dma((nz // 2, 2)),
+        dma,
+        dma,
         dma,
         dma,
         dma((2 * n,)),
@@ -450,7 +466,7 @@
     return pl.pallas_call(
         functools.partial(fused_kernel, n),
         out_shape=jax.ShapeDtypeStruct((toks, width // 2), bf16),
-        in_specs=[vmem] * 3 + [hbm] * 3 + [vmem] * 4,
+        in_specs=[hbm] + [vmem] * 2 + [hbm] * 6 + [vmem],
         out_specs=vmem,
         scratch_shapes=scratch,
         compiler_params=pltpu.CompilerParams(collective_id=0, has_side_effects=True),

time: 37.4 us -> 36.8 us (0.984)
  Pallas kernels: 35.7 us -> 35 us
    pallas_call x1, Pallas kernels: 35.7 us -> 35 us  [fused_local(): pl.pallas_call(functools.partial(fused_kernel, n), out_shape=jax.ShapeDty...]
where the time goes in v3:
time: 36.8 us; the launch traced here: 36.6 us
  Pallas kernels  35 us (95%)
  local copies, waits for them, and re-layouts  1.57 us (4%)
    pallas_call x1, Pallas kernels, fused_local(): pl.pallas_call(functools.partial(fused_kernel, n), out_shape=jax.ShapeDty...  35 us
    unnamed x1, local copies, waits for them, and re-layouts  1.57 us

profile of v3, /device:TPU:1, one launch (start us, length us, event | category | flops | bytes accessed | tf_op | source)
XLA Modules:
  0.0 36.6 jit_solution(16995903603952477217)
XLA Ops:
  0.0 35.0 %shard_map.100 = bf16[64,1024]{1,0:T(8,128)(2,1)} custom-call(bf16[64,2048]{1,0:T(8,128)(2,1)} %tok_hbm.1, s32[1,1,9]{2,1,0:T(1,128)} %chosen_ref.1, f32[1,1,9]{2,1,0:T(1,128)} %route_ref.1, bf16[2048,256]{1,0:T(8,128)(2,1)} %eg_hbm.1, bf16[2048,256]{1,0:T(8,128)(2,1)} %eu_hbm.1, bf16[256,2048]{1,0:T(8,128)(2,1)} %ed_hbm.1, bf16[256,256]{1,0:T(8,128)(2,1)} %dg_hbm.1, ...), custom_call_target="tpu_custom_call" | custom-call | tf_op jit(solution)/shard_map/pallas_call | solution.py:466
  35.0 1.6 %copy.12 = bf16[64,1024]{1,0:T(8,128)(2,1)} copy(bf16[64,1024]{1,0:T(8,128)(2,1)} %shard_map.100) | data formatting | bytes 262144

commit v4 on v3

--- a/solution.py
+++ b/solution.py
@@ -280,22 +280,22 @@
     gate = project(eg)
     up = project(eu)
     act = (gate / (1.0 + jnp.exp(-gate)) * up).astype(bf16)
+    for d in range(1, nz):
+        pcopies[d - 1].wait_recv()
+        sums = [sums[i] + part_recv[d - 1, i].astype(f32) for i in range(2)]
+    dense_hidden = (sums[0] / (1.0 + jnp.exp(-sums[0])) * sums[1]).astype(bf16)
+    hid_all[0] = dense_hidden
+    hcopies = []
+    for d in range(1, nz):
+        hcopies.append(
+            remote(hid_all.at[0], hid_all.at[d], h_send.at[d], h_recv.at[d], line(d), tp)
+        )
+
     loads[2].wait()
     off = pl.ds(pl.multiple_of(sib * halfw, halfw), halfw)
     keep = pl.ds(pl.multiple_of(tp * halfw, halfw), halfw)
     half_send[...] = jnp.dot(act, ed[:, off], preferred_element_type=f32).astype(bf16)
     scopy = remote(half_send, half_recv, s_send, s_recv, ep, sib)
-
-    for d in range(1, nz):
-        pcopies[d - 1].wait_recv()
-        sums = [sums[i] + part_recv[d - 1, i].astype(f32) for i in range(2)]
-    dense_hidden = (sums[0] / (1.0 + jnp.exp(-sums[0])) * sums[1]).astype(bf16)
-    hid_all[0] = dense_hidden
-    hcopies = []
-    for d in range(1, nz):
-        hcopies.append(
-            remote(hid_all.at[0], hid_all.at[d], h_send.at[d], h_recv.at[d], line(d), tp)
-        )
 
     own_half = jnp.dot(act, ed[:, keep], preferred_element_type=f32).astype(bf16)
     scopy.wait_recv()

time: 36.8 us -> 36.5 us (level)
  no operation moved by 1% of the time
where the time goes in v4:
time: 36.5 us; the launch traced here: 36.3 us
  Pallas kernels  34.7 us (95%)
  local copies, waits for them, and re-layouts  1.57 us (4%)
    pallas_call x1, Pallas kernels, fused_local(): pl.pallas_call(functools.partial(fused_kernel, n), out_shape=jax.ShapeDty...  34.7 us
    unnamed x1, local copies, waits for them, and re-layouts  1.57 us

profile of v4, /device:TPU:1, one launch (start us, length us, event | category | flops | bytes accessed | tf_op | source)
XLA Modules:
  0.0 36.3 jit_solution(1188892365969983427)
XLA Ops:
  0.0 34.7 %shard_map.100 = bf16[64,1024]{1,0:T(8,128)(2,1)} custom-call(bf16[64,2048]{1,0:T(8,128)(2,1)} %tok_hbm.1, s32[1,1,9]{2,1,0:T(1,128)} %chosen_ref.1, f32[1,1,9]{2,1,0:T(1,128)} %route_ref.1, bf16[2048,256]{1,0:T(8,128)(2,1)} %eg_hbm.1, bf16[2048,256]{1,0:T(8,128)(2,1)} %eu_hbm.1, bf16[256,2048]{1,0:T(8,128)(2,1)} %ed_hbm.1, bf16[256,256]{1,0:T(8,128)(2,1)} %dg_hbm.1, ...), custom_call_target="tpu_custom_call" | custom-call | tf_op jit(solution)/shard_map/pallas_call | solution.py:466
  34.7 1.6 %copy.12 = bf16[64,1024]{1,0:T(8,128)(2,1)} copy(bf16[64,1024]{1,0:T(8,128)(2,1)} %shard_map.100) | data formatting | bytes 262144
